TPU v7x, 32 devices: a whole 2x2x4 slice. The times are simulated.
32 devices in a mesh: ep: 4 (over z), tp: 8 (over y, x, core).
Axes of the slice: x: 2, y: 2, z: 4, core: 2. Of those that a mesh axis runs over, the one named last changes fastest.
Arguments:
- tokens: bfloat16 [256, 4096], P('ep', 'tp'), may hold values from -24 to 24, as said below
- state_real: float32 [256, 128, 64], P('ep', 'tp'), may hold values from -3 to 3
- state_imag: float32 [256, 128, 64], P('ep', 'tp'), may hold values from -3 to 3
- mix_gain: bfloat16 [4096], replicated, may hold values from 0.099609375 to 1.8984375
- in_weight: bfloat16 [2048, 4096], P('tp'), may hold values from -0.09375 to 0.09375
- eig_real: float32 [128, 64], P('tp'), may hold values from -1 to -0.1
- eig_imag: float32 [128, 64], P('tp'), may hold values from 0 to 200
- log_step: float32 [128], P('tp'), may hold values from -4 to 0
- input_real: float32 [128, 64, 16], P('tp'), may hold values from -1 to 1
- input_imag: float32 [128, 64, 16], P('tp'), may hold values from -1 to 1
- output_matrix_real: float32 [128, 16, 64], P('tp'), may hold values from -0.5 to 0.5
- output_matrix_imag: float32 [128, 16, 64], P('tp'), may hold values from -0.5 to 0.5
- skip_weight: float32 [2048], P('tp'), may hold values from -3 to 3
- glu_weight: bfloat16 [2048, 2048], P('tp'), may hold values from -0.375 to 0.375
- glu_bias: float32 [2048], P('tp'), may hold values from -3 to 3
- out_weight: bfloat16 [2048, 4096], P('tp'), may hold values from -0.25 to 0.25
- moe_gain: bfloat16 [4096], replicated, may hold values from 0.099609375 to 1.8984375
- routes: int32 [256, 2], P('ep'), may hold values from 0 to 7, all different within a row; in each aligned block of 64 rows (0 to 63, 64 to 127, ...) at most 24 rows name the same one
- route_weight: float32 [256, 2], P('ep'), may hold values from 0.2 to 1
- gate_weight: bfloat16 [8, 2048, 4096], P('ep', 'tp'), may hold values from -0.09375 to 0.09375
- up_weight: bfloat16 [8, 2048, 4096], P('ep', 'tp'), may hold values from -0.09375 to 0.09375
- down_weight: bfloat16 [8, 2048, 4096], P('ep', 'tp'), may hold values from -0.125 to 0.125
Outputs:
- result: bfloat16 [256, 4096], P('ep', 'tp')
- updated_state_real: float32 [256, 128, 64], P('ep', 'tp')
- updated_state_imag: float32 [256, 128, 64], P('ep', 'tp')
Inputs may be any that keep to these rules, and one draw needn't show every extreme that they name: `routes`: each row names 2 different experts. Among the rows of one index of ep, no expert is named by more than 24 rows, a bound that some expert reaches in some such blocks. `tokens`: feature blocks of the stream have scales that differ by up to a factor of ten.
All inputs are finite; a program needn't handle non-finite values.
Results may differ from a plain program's by a relative error of at most 0.013.
Values may be sent and summed in bfloat16 or wider, within the bound.
A program may use at most 64 MiB of HBM per device.

v0:
```python
import jax
import jax.numpy as jnp
from jax import lax
from jax.sharding import PartitionSpec as P

norm_eps = 1e-06


def ssm_step(
    driven,
    state_real,
    state_imag,
    eig_real,
    eig_imag,
    log_step,
    input_real,
    input_imag,
    output_matrix_real,
    output_matrix_imag,
    skip_weight,
):
    highest_precision = lax.Precision.HIGHEST
    count_of_rows = driven.shape[0]
    groups = eig_real.shape[0]
    group_width = input_real.shape[2]
    time_step = jnp.exp(log_step)[:, None]
    magnitude = jnp.exp(eig_real * time_step)
    angle_now = eig_imag * time_step
    bar_real = magnitude * jnp.cos(angle_now)
    bar_imag = magnitude * jnp.sin(angle_now)
    modulus = eig_real * eig_real + eig_imag * eig_imag
    fac_real = ((bar_real - 1.0) * eig_real + bar_imag * eig_imag) / modulus
    fac_imag = (bar_imag * eig_real - (bar_real - 1.0) * eig_imag) / modulus
    ib_real = fac_real[..., None] * input_real - fac_imag[..., None] * input_imag
    ib_imag = fac_real[..., None] * input_imag + fac_imag[..., None] * input_real
    grouped = driven.astype(jnp.float32).reshape(count_of_rows, groups, group_width)
    push_real = jnp.einsum("gpc,ngc->ngp", ib_real, grouped, precision=highest_precision)
    push_imag = jnp.einsum("gpc,ngc->ngp", ib_imag, grouped, precision=highest_precision)
    updated_state_real = bar_real[None] * state_real - bar_imag[None] * state_imag + push_real
    updated_state_imag = bar_real[None] * state_imag + bar_imag[None] * state_real + push_imag
    state_readout = jnp.einsum(
        "jiy,sjy->sji", output_matrix_real, updated_state_real, precision=highest_precision
    ) - jnp.einsum(
        "jiy,sjy->sji", output_matrix_imag, updated_state_imag, precision=highest_precision
    )
    state_readout = state_readout.reshape(count_of_rows, groups * group_width) + skip_weight[
        None, :
    ] * driven.astype(jnp.float32)
    activated = jax.nn.gelu(state_readout).astype(jnp.bfloat16)
    return (updated_state_real, updated_state_imag, activated)


def local(
    tokens,
    state_real,
    state_imag,
    mix_gain,
    in_weight,
    eig_real,
    eig_imag,
    log_step,
    input_real,
    input_imag,
    output_matrix_real,
    output_matrix_imag,
    skip_weight,
    glu_weight,
    glu_bias,
    out_weight,
    moe_gain,
    routes,
    route_weight,
    gate_weight,
    up_weight,
    down_weight,
):
    count_of_rows = tokens.shape[0]
    n_ep = lax.axis_size("ep")
    width_tp = lax.axis_size("tp")
    whole_rows = lax.all_gather(tokens, "tp", axis=1, tiled=True)
    whole_float = whole_rows.astype(jnp.float32)
    first_scale = lax.rsqrt(jnp.mean(whole_float * whole_float, axis=1, keepdims=True) + norm_eps)
    normed = (whole_float * first_scale * mix_gain.astype(jnp.float32)).astype(jnp.bfloat16)
    driven = jnp.einsum("rd,cd->rc", normed, in_weight, preferred_element_type=jnp.float32).astype(
        jnp.bfloat16
    )
    updated_state_real, updated_state_imag, activated = ssm_step(
        driven,
        state_real,
        state_imag,
        eig_real,
        eig_imag,
        log_step,
        input_real,
        input_imag,
        output_matrix_real,
        output_matrix_imag,
        skip_weight,
    )
    gate_pre = (
        jnp.einsum(
            "rc,oc->ro",
            lax.all_gather(activated, "tp", axis=1, tiled=True),
            glu_weight,
            preferred_element_type=jnp.float32,
        )
        + glu_bias
    )
    glued = (activated.astype(jnp.float32) * jax.nn.sigmoid(gate_pre)).astype(jnp.bfloat16)
    partial_value = jnp.dot(glued, out_weight, preferred_element_type=jnp.float32)
    mixed = lax.psum_scatter(
        partial_value.astype(jnp.bfloat16), "tp", scatter_dimension=1, tiled=True
    ).astype(jnp.float32)
    residual = (tokens.astype(jnp.float32) + mixed).astype(jnp.bfloat16)
    resid_float = residual.astype(jnp.float32)
    exp_dev = gate_weight.shape[0]
    experts = exp_dev * n_ep
    top_count = routes.shape[1]
    capacity = max(2, (3 * top_count * count_of_rows + 2 * experts - 1) // (2 * experts))
    chosen = routes.reshape(-1)
    onehot = (chosen[:, None] == jnp.arange(experts, dtype=jnp.int32)[None, :]).astype(jnp.int32)
    rank_index = jnp.sum((jnp.cumsum(onehot, axis=0) - onehot) * onehot, axis=1)
    slot_index = (chosen * capacity + rank_index).reshape(count_of_rows, top_count)
    slots_all = experts * capacity
    choose = slot_index[:, :, None] == jnp.arange(slots_all, dtype=jnp.int32)[None, None, :]
    dispatch = jnp.sum(choose.astype(jnp.float32), axis=1).astype(jnp.bfloat16)
    local_sq = jnp.sum(resid_float * resid_float, axis=1)
    total_sq = lax.psum(local_sq, "tp")
    dim_full = residual.shape[1] * width_tp
    second_scale = lax.rsqrt(total_sq[:, None] / dim_full + norm_eps)
    gain_part = lax.dynamic_slice_in_dim(
        moe_gain, lax.axis_index("tp") * residual.shape[1], residual.shape[1], 0
    )
    expert_in = (resid_float * second_scale * gain_part.astype(jnp.float32)).astype(jnp.bfloat16)
    packed = jnp.einsum(
        "rs,rd->sd", dispatch, expert_in, preferred_element_type=jnp.float32
    ).astype(jnp.bfloat16)
    packed = packed.reshape(n_ep, exp_dev * capacity, residual.shape[1])
    arrived = lax.all_to_all(packed, "ep", split_axis=0, concat_axis=0, tiled=True)
    arrived = arrived.reshape(n_ep, exp_dev, capacity, residual.shape[1])
    fragment = lax.all_gather(arrived, "tp", axis=3, tiled=True)
    gate_part = jnp.einsum(
        "necd,efd->necf", fragment, gate_weight, preferred_element_type=jnp.float32
    )
    up_part = jnp.einsum("necd,efd->necf", fragment, up_weight, preferred_element_type=jnp.float32)
    hidden_width = (jax.nn.silu(gate_part) * up_part).astype(jnp.bfloat16)
    partial_out = jnp.einsum(
        "necf,efd->necd", hidden_width, down_weight, preferred_element_type=jnp.float32
    )
    summed = lax.psum_scatter(
        partial_out.astype(jnp.bfloat16), "tp", scatter_dimension=3, tiled=True
    )
    summed = summed.reshape(n_ep, exp_dev * capacity, summed.shape[3])
    returned = lax.all_to_all(summed, "ep", split_axis=0, concat_axis=0, tiled=True)
    returned = returned.reshape(slots_all, returned.shape[2])
    gathered_k = jnp.einsum(
        "rks,sd->rkd", choose.astype(jnp.bfloat16), returned, preferred_element_type=jnp.float32
    )
    result = (resid_float + jnp.sum(route_weight[..., None] * gathered_k, axis=1)).astype(
        jnp.bfloat16
    )
    return (result, updated_state_real, updated_state_imag)


def solution(mesh):
    return jax.shard_map(
        local,
        mesh=mesh,
        in_specs=(
            P("ep", "tp"),
            P("ep", "tp", None),
            P("ep", "tp", None),
            P(),
            P("tp", None),
            P("tp", None),
            P("tp", None),
            P("tp"),
            P("tp", None, None),
            P("tp", None, None),
            P("tp", None, None),
            P("tp", None, None),
            P("tp"),
            P("tp", None),
            P("tp"),
            P("tp", None),
            P(),
            P("ep", None),
            P("ep", None),
            P("ep", "tp", None),
            P("ep", "tp", None),
            P("ep", "tp", None),
        ),
        out_specs=(P("ep", "tp"), P("ep", "tp", None), P("ep", "tp", None)),
        check_vma=False,
    )
```

profile of v0, /device:TPU:0, one launch (start us, length us, event | category | flops | bytes accessed | tf_op | source)
XLA Modules:
  0.0 198.0 jit_solution(15513446187685909442)
XLA Ops:
  7.2 0.0 copy-start
  7.2 0.0 copy-start.8
  7.2 0.0 copy-start.9
  7.2 0.0 copy-start.4
  7.2 0.0 copy-start.5
  7.2 0.0 copy-start.1
  7.2 0.0 reduce-scatter.3.cloned.1.call-start
  7.3 0.8 exp.13
  8.1 0.7 convert_element_type.73
  8.8 11.6 %all_gather.9 = bf16[64,4096]{1,0:T(8,128)(2,1)S(1)} all-gather(bf16[64,512]{1,0:T(8,128)(2,1)} %param.22), channel_id=1, replica_groups=mesh['ep'=4,'tp'=8] {'tp'}, dimensions={1}, use_global_device_ids=true | all-gather | bytes 589824 | tf_op jit(solution)/shard_map/all_gather | solution.py:80
  20.4 0.2 fusion.27
  20.7 2.4 %convolution_convert_fusion.3 = bf16[64,256]{1,0:T(8,128)(2,1)S(1)} fusion(bf16[256,4096]{1,0:T(8,128)(2,1)} %param.26, bf16[64,4096]{1,0:T(8,128)(2,1)S(1)} %all_gather.9, f32[4096]{0:T(1024)S(1)} %convert_element_type.73, f32[64]{0:T(128)S(1)} %add_rsqrt_fusion.1), kind=kOutput, calls=%fused_computation.29 | convolution fusion | flops 135282688 | bytes 2670848 | tf_op jit(solution)/shard_map/rd,cd->rc/dot_general | solution.py:84
  23.0 0.1 copy.54
  23.2 0.0 copy-done.8
  23.2 0.0 copy-done.9
  23.2 0.0 copy-start.7
  23.2 0.1 fusion.66
  23.3 0.0 copy-done.4
  23.3 0.0 copy-done.5
  23.3 0.0 copy-done.1
  23.3 0.0 copy-start.6
  23.4 1.7 fusion.6
  25.1 0.0 copy-start.11
  25.1 0.0 copy-start.12
  25.1 1.9 fusion.7
  27.0 0.0 copy-done.7
  27.0 0.9 fusion.69
  27.9 0.0 copy-done.6
  27.9 0.9 convolution_subtract_fusion
  28.9 0.1 copy.57
  29.0 0.0 copy-done.11
  29.0 9.5 %all_gather.10 = bf16[64,2048]{1,0:T(8,128)(2,1)S(1)} all-gather(bf16[64,256]{1,0:T(8,128)(2,1)S(1)} %fusion.50), channel_id=1, replica_groups=mesh['ep'=4,'tp'=8] {'tp'}, dimensions={1}, use_global_device_ids=true | all-gather | bytes 294912 | tf_op jit(solution)/shard_map/all_gather | solution.py:103
  38.6 3.4 %convolution_convert_fusion.1 = bf16[64,4096]{1,0:T(8,128)(2,1)} fusion(bf16[256,4096]{1,0:T(8,128)(2,1)S(1)} %copy-done, bf16[64,2048]{1,0:T(8,128)(2,1)S(1)} %all_gather.10, bf16[256,2048]{1,0:T(8,128)(2,1)} %param.35, bf16[64,256]{1,0:T(8,128)(2,1)S(1)} %fusion.50, f32[256]{0:T(256)S(1)} %copy-done.12), kind=kOutput, calls=%fused_computation.2 | convolution fusion | flops 201703424 | bytes 3965952 | tf_op jit(solution)/shard_map/dot_general | solution.py:110
  42.0 0.0 reduce-scatter.3.cloned.1.call-update
  42.0 0.0 all-gather.2.cloned.1.call-start
  42.1 0.1 copy.58
  42.2 0.1 eq.28
  42.3 0.1 fusion.55
  42.4 0.2 reduce_window_sum.11
  42.6 0.2 select_reduce_fusion
  42.8 0.1 reduce_sum.49
  42.9 0.1 copy.59
  43.0 0.8 dynamic-slice_convert_fusion
  43.7 0.1 convert_reduce_fusion
  43.8 32.7 %reduce-scatter.3.cloned.1.call-done = bf16[64,512]{1,0:T(8,128)(2,1)} async-done(((bf16[64,4096]{1,0:T(8,128)(2,1)}), bf16[64,512]{1,0:T(8,128)(2,1)}) %reduce-scatter.3.cloned.1.call-update) | async-done | bytes 65552 | tf_op jit(solution)/shard_map/reduce_scatter | solution.py:111
  76.6 1.0 fusion.33
  77.5 12.1 %psum.7 = f32[64]{0:T(128)S(1)} all-reduce(f32[64]{0:T(128)S(1)} %fusion.33), channel_id=1, replica_groups=mesh['ep'=4,'tp'=8] {'tp'}, use_global_device_ids=true, to_apply=%region_6.7 | all-reduce | flops 64 | bytes 512 | tf_op jit(solution)/shard_map/psum | solution.py:128
  89.7 1.1 convolution_convert_fusion.2
  90.8 11.8 %all_to_all.10 = bf16[4,48,512]{2,1,0:T(8,128)(2,1)S(1)} all-to-all(bf16[4,48,512]{2,1,0:T(8,128)(2,1)S(1)} %bitcast.69), channel_id=1, replica_groups=mesh['ep'=4,'tp'=8] {'ep'}, dimensions={0} | all-to-all | bytes 393216 | tf_op jit(solution)/shard_map/all_to_all | solution.py:139
  102.5 0.7 copy.60
  103.2 0.0 all-gather.2.cloned.1.call-update
  103.3 0.0 reduce-scatter.5.cloned.1.call-start
  103.3 23.8 %all-gather.2.cloned.1.call-done = bf16[4,2,24,4096]{3,2,0,1:T(8,128)(2,1)} async-done(((bf16[4,2,24,512]{3,2,0,1:T(8,128)(2,1)}), bf16[4,2,24,4096]{3,2,0,1:T(8,128)(2,1)}) %all-gather.2.cloned.1.call-update) | async-done | bytes 1572880 | tf_op jit(solution)/shard_map/all_gather | solution.py:141
  127.1 4.1 %fusion.9 = f32[4,2,24,256]{3,2,0,1:T(8,128)S(1)} fusion(bf16[4,2,24,4096]{3,2,0,1:T(8,128)(2,1)} %all-gather.2.cloned.1.call-done, bf16[2,256,4096]{2,1,0:T(8,128)(2,1)} %param.41), kind=kOutput, calls=%fused_computation.17 | convolution fusion | flops 402653184 | bytes 5963776 | tf_op jit(solution)/shard_map/necd,efd->necf/dot_general | solution.py:142
  131.2 7.3 %fusion = bf16[4,2,24,4096]{3,2,0,1:T(8,128)(2,1)} fusion(bf16[2,256,4096]{2,1,0:T(8,128)(2,1)} %param.43, bf16[4,2,24,4096]{3,2,0,1:T(8,128)(2,1)} %all-gather.2.cloned.1.call-done, bf16[2,256,4096]{2,1,0:T(8,128)(2,1)} %param.42, f32[4,2,24,256]{3,2,0,1:T(8,128)S(1)} %fusion.9), kind=kOutput, calls=%fused_computation.1 | convolution fusion | flops 806387712 | bytes 11730944 | tf_op jit(solution)/shard_map/necf,efd->necd/dot_general | solution.py:147
  138.5 0.0 reduce-scatter.5.cloned.1.call-update
  138.6 38.5 %reduce-scatter.5.cloned.1.call-done = bf16[4,2,24,512]{3,2,0,1:T(8,128)(2,1)} async-done(((bf16[4,2,24,4096]{3,2,0,1:T(8,128)(2,1)}), bf16[4,2,24,512]{3,2,0,1:T(8,128)(2,1)}) %reduce-scatter.5.cloned.1.call-update) | async-done | bytes 196624 | tf_op jit(solution)/shard_map/reduce_scatter | solution.py:150
  177.1 1.6 copy.61
  178.7 4.6 %all-to-all-start.1 = ((bf16[4,48,512]{2,1,0:T(8,128)(2,1)}), bf16[4,48,512]{2,1,0:T(8,128)(2,1)S(1)}, u32[]{:S(2)}, u32[]{:S(2)}) async-start(bf16[4,48,512]{2,1,0:T(8,128)(2,1)} %bitcast.16), calls=%async_computation.3 | async-start | bytes 393216 | tf_op jit(solution)/shard_map/all_to_all | solution.py:154
  183.3 1.1 copy.62
  184.4 1.1 copy.63
  185.5 5.1 %all-to-all-done.1 = bf16[4,48,512]{2,1,0:T(8,128)(2,1)S(1)} async-done(((bf16[4,48,512]{2,1,0:T(8,128)(2,1)}), bf16[4,48,512]{2,1,0:T(8,128)(2,1)S(1)}, u32[]{:S(2)}, u32[]{:S(2)}) %all-to-all-start.1) | async-done | bytes 196640 | tf_op jit(solution)/shard_map/all_to_all | solution.py:154
  190.6 0.2 fusion.8
  190.8 0.7 fusion.36
  (14 shorter events, 0.1 us)
Async XLA Ops:
  7.2 31.4 %copy-start = (bf16[256,4096]{1,0:T(8,128)(2,1)S(1)}, bf16[256,4096]{1,0:T(8,128)(2,1)}, u32[]{:S(2)}) copy-start(bf16[256,4096]{1,0:T(8,128)(2,1)} %param.37) | copy-start | bytes 6291460
  7.2 16.0 %copy-start.8 = (f32[16,64]{1,0:T(8,128)S(1)}, f32[16,64]{1,0:T(8,128)}, u32[]{:S(2)}) copy-start(f32[16,64]{1,0:T(8,128)} %param.28) | copy-start | bytes 12292
  7.2 16.0 %copy-start.9 = (f32[16,64]{1,0:T(8,128)S(1)}, f32[16,64]{1,0:T(8,128)}, u32[]{:S(2)}) copy-start(f32[16,64]{1,0:T(8,128)} %param.27) | copy-start | bytes 12292
  7.2 16.1 %copy-start.4 = (f32[16,64,16]{1,2,0:T(8,128)S(1)}, f32[16,64,16]{1,2,0:T(8,128)}, u32[]{:S(2)}) copy-start(f32[16,64,16]{1,2,0:T(8,128)} %param.31) | copy-start | bytes 196612
  7.2 16.1 %copy-start.5 = (f32[16,64,16]{1,2,0:T(8,128)S(1)}, f32[16,64,16]{1,2,0:T(8,128)}, u32[]{:S(2)}) copy-start(f32[16,64,16]{1,2,0:T(8,128)} %param.30) | copy-start | bytes 196612
  7.2 16.1 %copy-start.1 = (f32[64,16,64]{2,1,0:T(8,128)S(1)}, f32[64,16,64]{2,1,0:T(8,128)}, u32[]{:S(2)}) copy-start(f32[64,16,64]{2,1,0:T(8,128)} %param.24) | copy-start | bytes 786436
  7.2 69.3 %reduce-scatter.3.cloned.1.call-start = ((), (), s32[]{:S(2)}) async-start(), calls=%async_computation.4 | async-start | bytes 589824 | tf_op jit(solution)/shard_map/reduce_scatter | solution.py:111
  23.2 3.8 %copy-start.7 = (f32[16,16,64]{2,1,0:T(8,128)S(1)}, f32[16,16,64]{2,1,0:T(8,128)}, u32[]{:S(2)}) copy-start(f32[16,16,64]{2,1,0:T(8,128)} %param.32) | copy-start | bytes 196612
  23.3 4.6 %copy-start.6 = (f32[16,16,64]{2,1,0:T(8,128)S(1)}, f32[16,16,64]{2,1,0:T(8,128)}, u32[]{:S(2)}) copy-start(f32[16,16,64]{2,1,0:T(8,128)} %param.33) | copy-start | bytes 196612
  25.1 3.9 %copy-start.11 = (f32[256]{0:T(256)S(1)}, f32[256]{0:T(256)}, u32[]{:S(2)}) copy-start(f32[256]{0:T(256)} %param.34) | copy-start | bytes 3076
  25.1 13.4 %copy-start.12 = (f32[256]{0:T(256)S(1)}, f32[256]{0:T(256)}, u32[]{:S(2)}) copy-start(f32[256]{0:T(256)} %param.36) | copy-start | bytes 3076
  38.6 3.5 %copy-start.10 = (s32[64,2]{0,1:T(2,128)S(1)}, s32[64,2]{0,1:T(2,128)}, u32[]{:S(2)}) copy-start(s32[64,2]{0,1:T(2,128)} %param.39) | copy-start | bytes 1540
  38.6 38.0 %copy-start.2 = (bf16[64,512]{1,0:T(8,128)(2,1)S(1)}, bf16[64,512]{1,0:T(8,128)(2,1)}, u32[]{:S(2)}) copy-start(bf16[64,512]{1,0:T(8,128)(2,1)} %param.22) | copy-start | bytes 196612
  42.0 85.1 %all-gather.2.cloned.1.call-start = ((), (), s32[]{:S(2)}) async-start(), calls=%async_computation.5 | async-start | bytes 1769472 | tf_op jit(solution)/shard_map/all_gather | solution.py:141
  103.3 73.8 %reduce-scatter.5.cloned.1.call-start = ((), (), s32[]{:S(2)}) async-start(), calls=%async_computation.6 | async-start | bytes 1769472 | tf_op jit(solution)/shard_map/reduce_scatter | solution.py:150
  138.5 52.0 %copy-start.13 = (f32[64,2]{0,1:T(2,128)S(1)}, f32[64,2]{0,1:T(2,128)}, u32[]{:S(2)}) copy-start(f32[64,2]{0,1:T(2,128)} %param.40) | copy-start | bytes 1540
  138.5 52.3 %copy-start.3 = (bf16[64,512]{1,0:T(8,128)(2,1)S(1)}, bf16[64,512]{1,0:T(8,128)(2,1)}, u32[]{:S(2)}) copy-start(bf16[64,512]{1,0:T(8,128)(2,1)} %reduce-scatter.3.cloned.1.call-done) | copy-start | bytes 196612
  178.7 11.9 %all-to-all-start.1 = ((bf16[4,48,512]{2,1,0:T(8,128)(2,1)}), bf16[4,48,512]{2,1,0:T(8,128)(2,1)S(1)}, u32[]{:S(2)}, u32[]{:S(2)}) async-start(bf16[4,48,512]{2,1,0:T(8,128)(2,1)} %bitcast.16), calls=%async_computation.3 | async-start | bytes 393216 | tf_op jit(solution)/shard_map/all_to_all | solution.py:154
Sparse Core Ops, SparseCore 0:
  42.1 34.3 reduce-scatter.2
  103.4 23.6 all-gather.1
  138.7 38.3 reduce-scatter.4
where the time goes:
time: 199 us; the launch traced here: 198 us
  waiting for transfers between devices  100 us (50%)
  blocking collectives  45.1 us (23%)
  matrix products  24 us (12%)
  between operations  14 us (7%)
  local copies, waits for them, and re-layouts  6.04 us (3%)
  starting transfers between devices  4.73 us (2%)
  other arithmetic  4.04 us (2%)
    reduce_scatter x1, waiting for transfers between devices, local(): lax.psum_scatter(partial_out.astype(jnp.bfloat16), 'tp', scatter_dimensio...  38.5 us
    reduce_scatter x1, waiting for transfers between devices, local(): lax.psum_scatter(partial_value.astype(jnp.bfloat16), 'tp', scatter_dimens...  32.7 us
    all_gather x1, waiting for transfers between devices, local(): fragment = lax.all_gather(arrived, 'tp', axis=3, tiled=True)  23.8 us
    psum x1, blocking collectives, local(): total_sq = lax.psum(local_sq, 'tp')  12.1 us
    all_to_all x1, blocking collectives, local(): lax.all_to_all(packed, 'ep', split_axis=0, concat_axis=0, tiled=True)  11.8 us
    all_gather x1, blocking collectives, local(): whole_rows = lax.all_gather(tokens, 'tp', axis=1, tiled=True)  11.6 us
    all_gather x1, blocking collectives, local(): lax.all_gather(activated, 'tp', axis=1, tiled=True)  9.53 us
    dot_general x1, matrix products, local(): jnp.einsum('necf,efd->necd', hidden_width, down_weight, preferred_element...  7.3 us
  transfers between devices with their start and end apart: 4, of which 4 were waited for; matrix products, arithmetic and copies ran while one was open for 2% of the time, Pallas kernels for 0%

commit v1 on v0

v1 whole, which is shorter than its diff:
```python
import functools

import jax
import jax.numpy as jnp
from jax import lax
from jax.experimental import pallas as pl
from jax.experimental.pallas import tpu as pltpu
from jax.sharding import PartitionSpec as P

norm_eps = 1e-06
MESH = pl.DeviceIdType.MESH
F32 = jnp.float32
BF16 = jnp.bfloat16


def dot_nt(a, b):
    return lax.dot_general(a, b, (((1,), (1,)), ((), ())), preferred_element_type=F32)


def dot_nn(a, b):
    return lax.dot_general(a, b, (((1,), (0,)), ((), ())), preferred_element_type=F32)


def layer_kernel(
    n_ep, n_tp, capacity,
    tok, mix_gain, moe_gain, routes, route_weight, eig_real, eig_imag, log_step,
    in_real, in_imag, out_real, out_imag, skip_weight, glu_bias,
    state_real, state_imag, in_weight, glu_weight, out_weight, gate_weight, up_weight, down_weight,
    result, new_real, new_imag,
    tok_all, act_all, sib_send_a, sib_recv_a, rem_send_a, rem_recv_a,
    ep_send, frag, acc, sib_send_b, sib_recv_b, rem_send_b, rem_recv_b, ret_send, ret,
    state_r, state_i, next_r, next_i, pad_r, pad_i, w_in, w_glu, w_out, w_gate, w_up, w_down,
    load_sem, store_sem, s1, r1, s2, r2, s3, r3, s4, r4, s5, r5, s6, r6, s7, r7, s8, r8, s9, r9,
):
    e = lax.axis_index("ep")
    t = lax.axis_index("tp")
    core = lax.rem(t, 2)
    chip = t // 2
    sib = t + 1 - 2 * core
    chips = n_tp // 2
    rows, feat = tok.shape
    width = in_weight.shape[0]
    groups, states = eig_real.shape
    group_width = in_real.shape[1]
    exp_dev = gate_weight.shape[0]
    per_ep = exp_dev * capacity
    slots = n_ep * per_ep
    dim = feat * n_tp

    loads = []
    for at, (src, dst) in enumerate((
        (in_weight, w_in), (state_real, state_r), (state_imag, state_i), (glu_weight, w_glu),
        (out_weight, w_out), (gate_weight, w_gate), (up_weight, w_up), (down_weight, w_down),
    )):
        load = pltpu.make_async_copy(src, dst, load_sem.at[at])
        load.start()
        loads.append(load)

    def remote_chip(j):
        return lax.rem(chip + j, chips)

    barrier = pltpu.get_barrier_semaphore()
    greeted = [(e, sib)]
    greeted += [(e, 2 * remote_chip(j) + core) for j in range(1, chips)]
    greeted += [(lax.rem(e + k, n_ep), t) for k in range(1, n_ep)]
    for other in greeted:
        pl.semaphore_signal(barrier, inc=1, device_id=other, device_id_type=MESH)
    pl.semaphore_wait(barrier, len(greeted))

    sends = []

    def send(src, dst, send_sem, recv_sem, target):
        copy = pltpu.make_async_remote_copy(
            src_ref=src, dst_ref=dst, send_sem=send_sem, recv_sem=recv_sem,
            device_id=target, device_id_type=MESH,
        )
        copy.start()
        sends.append(copy)

    def arrive(dst, send_sem, recv_sem):
        pltpu.make_async_remote_copy(
            src_ref=dst, dst_ref=dst, send_sem=send_sem, recv_sem=recv_sem,
            device_id=(e, sib), device_id_type=MESH,
        ).wait_recv()

    def gather_send(src, dst_at, ssem, rsem):
        for j in range(1, chips):
            send(src, dst_at(t), ssem(j), rsem(t), (e, 2 * remote_chip(j) + core))
        send(src, dst_at(t), ssem(0), rsem(t), (e, sib))

    gather_send(tok, lambda p: tok_all.at[p], lambda i: s1.at[i], lambda p: r1.at[p])

    spread = (
        lax.broadcasted_iota(jnp.int32, (group_width, width), 1) % group_width
        == lax.broadcasted_iota(jnp.int32, (group_width, width), 0)
    ).astype(F32).astype(BF16)
    own_group = (
        lax.broadcasted_iota(jnp.int32, (groups * states, width), 1) // group_width
        == lax.broadcasted_iota(jnp.int32, (groups * states, width), 0) // states
    )
    pad_r[...] = jnp.where(own_group, dot_nn(in_real[...].astype(BF16), spread), 0.0).astype(BF16)
    pad_i[...] = jnp.where(own_group, dot_nn(in_imag[...].astype(BF16), spread), 0.0).astype(BF16)
    square = lax.broadcasted_iota(jnp.int32, (groups, groups), 0) == lax.broadcasted_iota(
        jnp.int32, (groups, groups), 1
    )
    time_step = jnp.exp(jnp.sum(jnp.where(square, log_step[...], 0.0), axis=1, keepdims=True))
    e_r, e_i = eig_real[...], eig_imag[...]
    magnitude = jnp.exp(e_r * time_step)
    angle = e_i * time_step
    bar_r = magnitude * jnp.cos(angle)
    bar_i = magnitude * jnp.sin(angle)
    modulus = e_r * e_r + e_i * e_i
    fac_r = ((bar_r - 1.0) * e_r + bar_i * e_i) / modulus
    fac_i = (bar_i * e_r - (bar_r - 1.0) * e_i) / modulus

    experts = exp_dev * n_ep
    lane_expert = lax.broadcasted_iota(jnp.int32, (rows, experts), 1)
    route = routes[...]
    top = route.shape[1]
    picks = [(route[:, k : k + 1] == lane_expert).astype(F32) for k in range(top)]
    earlier = (
        lax.broadcasted_iota(jnp.int32, (rows, rows), 0) > lax.broadcasted_iota(jnp.int32, (rows, rows), 1)
    ).astype(F32).astype(BF16)
    prefix = dot_nn(earlier, sum(picks[1:], picks[0]).astype(BF16))
    lane_slot = lax.broadcasted_iota(jnp.int32, (rows, slots), 1)
    choose = []
    for k in range(top):
        rank = jnp.sum(prefix * picks[k], axis=1, keepdims=True).astype(jnp.int32)
        slot = route[:, k : k + 1] * capacity + rank
        choose.append((slot == lane_slot).astype(F32))
    dispatch = jnp.transpose(sum(choose[1:], choose[0])).astype(BF16)
    choose = [one.astype(BF16) for one in choose]

    def columns(p):
        return pl.ds(pl.multiple_of(p * feat, feat), feat)

    def in_piece(p, x, total, sq):
        xf = x.astype(F32)
        sq = sq + jnp.sum(xf * xf, axis=1, keepdims=True)
        y = (xf * mix_gain[:, columns(p)].astype(F32)).astype(BF16)
        return total + dot_nt(y, w_in[:, columns(p)]), sq

    loads[0].wait()
    total, sq = in_piece(t, tok[...], jnp.zeros((rows, width), F32), jnp.zeros((rows, 1), F32))
    arrive(tok_all.at[sib], s1.at[0], r1.at[sib])
    total, sq = in_piece(sib, tok_all[sib], total, sq)
    for j in range(1, chips):
        p = 2 * remote_chip(j) + core
        arrive(tok_all.at[p], s1.at[0], r1.at[p])
        send(tok_all.at[p], tok_all.at[p], s1.at[chips + j - 1], r1.at[p], (e, sib))
        total, sq = in_piece(p, tok_all[p], total, sq)
    for j in range(1, chips):
        p = 2 * remote_chip(j) + 1 - core
        arrive(tok_all.at[p], s1.at[0], r1.at[p])
        total, sq = in_piece(p, tok_all[p], total, sq)
    driven = (total * lax.rsqrt(sq / dim + norm_eps)).astype(BF16)
    driven_f = driven.astype(F32)

    loads[1].wait()
    loads[2].wait()
    readout = skip_weight[...] * driven_f
    c_r, c_i = out_real[...], out_imag[...]
    row_group = lax.broadcasted_iota(jnp.int32, c_r.shape, 0) // group_width
    for g in range(groups):
        at = pl.ds(g, rows, stride=groups)
        part = slice(g * states, (g + 1) * states)
        push_r = dot_nt(driven, pad_r[part, :])
        push_i = dot_nt(driven, pad_i[part, :])
        old_r, old_i = state_r[at, :], state_i[at, :]
        br, bi = bar_r[g : g + 1, :], bar_i[g : g + 1, :]
        fr, fi = fac_r[g : g + 1, :], fac_i[g : g + 1, :]
        now_r = br * old_r - bi * old_i + (fr * push_r - fi * push_i)
        now_i = br * old_i + bi * old_r + (fr * push_i + fi * push_r)
        next_r[at, :] = now_r
        next_i[at, :] = now_i
        mine = row_group == g
        readout = readout + dot_nt(now_r.astype(BF16), jnp.where(mine, c_r, 0.0).astype(BF16))
        readout = readout - dot_nt(now_i.astype(BF16), jnp.where(mine, c_i, 0.0).astype(BF16))
    activated = jax.nn.gelu(readout).astype(BF16)

    act_all[t] = activated
    gather_send(act_all.at[t], lambda p: act_all.at[p], lambda i: s2.at[i], lambda p: r2.at[p])
    stores = []
    for at, (src, dst) in enumerate(((next_r, new_real), (next_i, new_imag))):
        store = pltpu.make_async_copy(src, dst, store_sem.at[at])
        store.start()
        stores.append(store)
    loads[3].wait()
    arrive(act_all.at[sib], s2.at[0], r2.at[sib])
    for j in range(1, chips):
        p = 2 * remote_chip(j) + core
        arrive(act_all.at[p], s2.at[0], r2.at[p])
        send(act_all.at[p], act_all.at[p], s2.at[chips + j - 1], r2.at[p], (e, sib))
    for j in range(1, chips):
        p = 2 * remote_chip(j) + 1 - core
        arrive(act_all.at[p], s2.at[0], r2.at[p])
    gate_pre = glu_bias[...] + jnp.zeros((rows, width), F32)
    for p in range(n_tp):
        gate_pre = gate_pre + dot_nt(act_all[p], w_glu[:, p * width : (p + 1) * width])
    glued = (activated.astype(F32) * jax.nn.sigmoid(gate_pre)).astype(BF16)

    def reduce_blocks(partial, sib_send, sib_recv, rem_send, rem_recv, ssem, rsem, ssem2, rsem2):
        order = list(range(1, chips)) + [0]
        for j in order:
            sib_send[j] = partial(2 * remote_chip(j) + 1 - core).astype(BF16)
            send(sib_send.at[j], sib_recv.at[j], ssem.at[j], rsem.at[j], (e, sib))
        for j in order[:-1]:
            p = 2 * remote_chip(j) + core
            value = partial(p)
            arrive(sib_recv.at[j], ssem.at[j], rsem.at[j])
            rem_send[j] = (value + sib_recv[j].astype(F32)).astype(BF16)
            send(rem_send.at[j], rem_recv.at[j], ssem2.at[j], rsem2.at[j], (e, p))
        value = partial(t)
        arrive(sib_recv.at[0], ssem.at[0], rsem.at[0])
        value = value + sib_recv[0].astype(F32)
        for j in order[:-1]:
            arrive(rem_recv.at[j], ssem2.at[j], rsem2.at[j])
            value = value + rem_recv[j].astype(F32)
        return value

    loads[4].wait()
    mixed = reduce_blocks(
        lambda p: dot_nn(glued, w_out[:, columns(p)]),
        sib_send_a, sib_recv_a, rem_send_a, rem_recv_a, s3, r3, s4, r4,
    )
    residual = (tok[...].astype(F32) + mixed).astype(BF16)

    packed = dot_nn(dispatch, residual).astype(BF16).reshape(n_ep, per_ep, feat)
    ep_send[...] = packed
    for k in range(1, n_ep):
        to = lax.rem(e + k, n_ep)
        send(ep_send.at[to], frag.at[t, e], s5.at[k], r5.at[e], (to, t))
    frag[t, e] = ep_send[e]
    sources = [lax.rem(e + n_ep - k, n_ep) for k in range(n_ep)]
    for k, source in enumerate(sources):
        if k:
            arrive(frag.at[t, source], s5.at[0], r5.at[source])
        gather_send(
            frag.at[t, source], lambda p: frag.at[p, source],
            lambda i: s6.at[i, k], lambda p: r6.at[p, source],
        )

    for load in loads[5:]:
        load.wait()

    def expert_piece(p, sq, first):
        xf = frag[p].reshape(slots, feat).astype(F32)
        y = (xf * moe_gain[:, columns(p)].astype(F32)).astype(BF16)
        for x in range(exp_dev):
            gate = dot_nt(y, w_gate[x, :, columns(p)])
            up = dot_nt(y, w_up[x, :, columns(p)])
            acc[2 * x] = gate if first else acc[2 * x] + gate
            acc[2 * x + 1] = up if first else acc[2 * x + 1] + up
        return sq + jnp.sum(xf * xf, axis=1, keepdims=True)

    sq = expert_piece(t, jnp.zeros((slots, 1), F32), True)
    for source in sources:
        arrive(frag.at[sib, source], s6.at[0, 0], r6.at[sib, source])
    sq = expert_piece(sib, sq, False)
    for j in range(1, chips):
        p = 2 * remote_chip(j) + core
        for k, source in enumerate(sources):
            arrive(frag.at[p, source], s6.at[0, 0], r6.at[p, source])
            send(frag.at[p, source], frag.at[p, source], s6.at[chips + j - 1, k], r6.at[p, source], (e, sib))
        sq = expert_piece(p, sq, False)
    for j in range(1, chips):
        p = 2 * remote_chip(j) + 1 - core
        for source in sources:
            arrive(frag.at[p, source], s6.at[0, 0], r6.at[p, source])
        sq = expert_piece(p, sq, False)

    second_scale = lax.rsqrt(sq / dim + norm_eps)
    hidden_of = []
    for x in range(exp_dev):
        slot_row = lax.broadcasted_iota(jnp.int32, acc.shape[1:], 0)
        mine = (slot_row % per_ep) // capacity == x
        hidden = jax.nn.silu(acc[2 * x] * second_scale) * (acc[2 * x + 1] * second_scale)
        hidden_of.append(jnp.where(mine, hidden, 0.0).astype(BF16))

    def down(p):
        value = dot_nn(hidden_of[0], w_down[0, :, columns(p)])
        for x in range(1, exp_dev):
            value = value + dot_nn(hidden_of[x], w_down[x, :, columns(p)])
        return value

    summed = reduce_blocks(
        down, sib_send_b, sib_recv_b, rem_send_b, rem_recv_b, s7, r7, s8, r8,
    ).astype(BF16)

    ret_send[...] = summed.reshape(n_ep, per_ep, feat)
    for k in range(1, n_ep):
        to = lax.rem(e + k, n_ep)
        send(ret_send.at[to], ret.at[e], s9.at[k], r9.at[e], (to, t))
    ret[e] = ret_send[e]
    for source in sources[1:]:
        arrive(ret.at[source], s9.at[0], r9.at[source])
    returned = ret[...].reshape(slots, feat)
    total = residual.astype(F32)
    weights = route_weight[...]
    for k in range(top):
        total = total + weights[:, k : k + 1] * dot_nn(choose[k], returned)
    result[...] = total.astype(BF16)

    for store in stores:
        store.wait()
    for copy in sends:
        copy.wait_send()


def local(
    tokens, state_real, state_imag, mix_gain, in_weight, eig_real, eig_imag, log_step,
    input_real, input_imag, output_matrix_real, output_matrix_imag, skip_weight,
    glu_weight, glu_bias, out_weight, moe_gain, routes, route_weight,
    gate_weight, up_weight, down_weight,
):
    rows, feat = tokens.shape
    n_ep = lax.axis_size("ep")
    n_tp = lax.axis_size("tp")
    chips = n_tp // 2
    groups, states, group_width = input_real.shape
    width = in_weight.shape[0]
    exp_dev, hidden, dim = gate_weight.shape
    experts = exp_dev * n_ep
    top_count = routes.shape[1]
    capacity = max(2, (3 * top_count * rows + 2 * experts - 1) // (2 * experts))
    per_ep = exp_dev * capacity
    slots = n_ep * per_ep
    vmem = pl.BlockSpec(memory_space=pltpu.VMEM)
    hbm = pl.BlockSpec(memory_space=pl.ANY)
    dma = pltpu.SemaphoreType.DMA
    state_shape = (rows * groups, states)
    outs = pl.pallas_call(
        functools.partial(layer_kernel, n_ep, n_tp, capacity),
        out_shape=(
            jax.ShapeDtypeStruct((rows, feat), BF16),
            jax.ShapeDtypeStruct(state_shape, F32),
            jax.ShapeDtypeStruct(state_shape, F32),
        ),
        in_specs=[vmem] * 14 + [hbm] * 8,
        out_specs=(vmem, hbm, hbm),
        scratch_shapes=[
            pltpu.VMEM((n_tp, rows, feat), BF16),
            pltpu.VMEM((n_tp, rows, width), BF16),
            pltpu.VMEM((chips, rows, feat), BF16),
            pltpu.VMEM((chips, rows, feat), BF16),
            pltpu.VMEM((chips, rows, feat), BF16),
            pltpu.VMEM((chips, rows, feat), BF16),
            pltpu.VMEM((n_ep, per_ep, feat), BF16),
            pltpu.VMEM((n_tp, n_ep, per_ep, feat), BF16),
            pltpu.VMEM((2 * exp_dev, slots, hidden), F32),
            pltpu.VMEM((chips, slots, feat), BF16),
            pltpu.VMEM((chips, slots, feat), BF16),
            pltpu.VMEM((chips, slots, feat), BF16),
            pltpu.VMEM((chips, slots, feat), BF16),
            pltpu.VMEM((n_ep, per_ep, feat), BF16),
            pltpu.VMEM((n_ep, per_ep, feat), BF16),
            pltpu.VMEM(state_shape, F32),
            pltpu.VMEM(state_shape, F32),
            pltpu.VMEM(state_shape, F32),
            pltpu.VMEM(state_shape, F32),
            pltpu.VMEM((groups * states, width), BF16),
            pltpu.VMEM((groups * states, width), BF16),
            pltpu.VMEM(in_weight.shape, BF16),
            pltpu.VMEM(glu_weight.shape, BF16),
            pltpu.VMEM(out_weight.shape, BF16),
            pltpu.VMEM(gate_weight.shape, BF16),
            pltpu.VMEM(up_weight.shape, BF16),
            pltpu.VMEM(down_weight.shape, BF16),
            dma((8,)),
            dma((2,)),
            dma((n_tp,)), dma((n_tp,)),
            dma((n_tp,)), dma((n_tp,)),
            dma((chips,)), dma((chips,)),
            dma((chips,)), dma((chips,)),
            dma((n_ep,)), dma((n_ep,)),
            dma((n_tp, n_ep)), dma((n_tp, n_ep)),
            dma((chips,)), dma((chips,)),
            dma((chips,)), dma((chips,)),
            dma((n_ep,)), dma((n_ep,)),
        ],
        compiler_params=pltpu.CompilerParams(
            collective_id=0, has_side_effects=True, vmem_limit_bytes=60 * 1024 * 1024
        ),
    )(
        tokens, mix_gain.reshape(1, dim), moe_gain.reshape(1, dim), routes, route_weight,
        eig_real, eig_imag, log_step.reshape(1, groups),
        input_real.reshape(groups * states, group_width),
        input_imag.reshape(groups * states, group_width),
        output_matrix_real.reshape(width, states), output_matrix_imag.reshape(width, states),
        skip_weight.reshape(1, width), glu_bias.reshape(1, width),
        state_real.reshape(state_shape), state_imag.reshape(state_shape),
        in_weight, glu_weight, out_weight, gate_weight, up_weight, down_weight,
    )
    result, new_real, new_imag = outs
    return result, new_real.reshape(state_real.shape), new_imag.reshape(state_imag.shape)


def solution(mesh):
    return jax.shard_map(
        local,
        mesh=mesh,
        in_specs=(
            P("ep", "tp"),
            P("ep", "tp", None),
            P("ep", "tp", None),
            P(),
            P("tp", None),
            P("tp", None),
            P("tp", None),
            P("tp"),
            P("tp", None, None),
            P("tp", None, None),
            P("tp", None, None),
            P("tp", None, None),
            P("tp"),
            P("tp", None),
            P("tp"),
            P("tp", None),
            P(),
            P("ep", None),
            P("ep", None),
            P("ep", "tp", None),
            P("ep", "tp", None),
            P("ep", "tp", None),
        ),
        out_specs=(P("ep", "tp"), P("ep", "tp", None), P("ep", "tp", None)),
        check_vma=False,
    )
```

time: 199 us -> 76.4 us (0.38)
  waiting for transfers between devices: 100 us -> 0 us
  Pallas kernels: 0 us -> 60.9 us
  blocking collectives: 45.1 us -> 0 us
  matrix products: 24 us -> 0 us
  between operations: 14 us -> 0.64 us
  local copies, waits for them, and re-layouts: 6.04 us -> 14.4 us
  starting transfers between devices: 4.73 us -> 0 us
  other arithmetic: 4.04 us -> 0 us
    reduce_scatter x2 -> x0, waiting for transfers between devices: 71.2 us -> none  [the longest x1 38.5 us: local(): lax.psum_scatter(partial_out.astype(jnp.bfloat16), 'tp', scatter_dimensio...]
    pallas_call x0 -> x1, Pallas kernels: none -> 60.9 us  [local(): pl.pallas_call(functools.partial(layer_kernel, n_ep, n_tp, capacity), out...]
    dot_general x10 -> x0, matrix products: 24 us -> none  [the longest x1 7.3 us: local(): jnp.einsum('necf,efd->necd', hidden_width, down_weight, preferred_element...]
    all_gather x1 -> x0, waiting for transfers between devices: 23.8 us -> none  [local(): fragment = lax.all_gather(arrived, 'tp', axis=3, tiled=True)]
    all_gather x2 -> x0, blocking collectives: 21.1 us -> none  [the longest x1 11.6 us: local(): whole_rows = lax.all_gather(tokens, 'tp', axis=1, tiled=True)]
    psum x1 -> x0, blocking collectives: 12.1 us -> none  [local(): total_sq = lax.psum(local_sq, 'tp')]
    all_to_all x1 -> x0, blocking collectives: 11.8 us -> none  [local(): lax.all_to_all(packed, 'ep', split_axis=0, concat_axis=0, tiled=True)]
    unnamed x31 -> x7, local copies, waits for them, and re-layouts: 2.37 us -> 11.8 us
  transfers between devices with their start and end apart: 4 -> 0, of which waited for: 4 -> 0; matrix products, arithmetic and copies ran while one was open for 2% -> 0% of each run, Pallas kernels for 0% -> 0%
where the time goes in v1:
time: 76.4 us; the launch traced here: 75.9 us
  Pallas kernels  60.9 us (80%)
  local copies, waits for them, and re-layouts  14.4 us (19%)
    pallas_call x1, Pallas kernels, local(): pl.pallas_call(functools.partial(layer_kernel, n_ep, n_tp, capacity), out...  60.9 us
    unnamed x7, local copies, waits for them, and re-layouts  11.8 us

profile of v1, /device:TPU:0, one launch (start us, length us, event | category | flops | bytes accessed | tf_op | source)
XLA Modules:
  0.0 75.9 jit_solution(8111238555541616006)
XLA Ops:
  0.6 1.3 %reshape.45.mix_gain = bf16[1,4096]{1,0:T(2,128)(2,1)} reshape(bf16[4096]{0:T(1024)(128)(2,1)} %param.25) | data formatting | bytes 16384 | tf_op jit(solution)/shard_map/reshape | solution.py:385
  1.9 1.3 %reshape.46.moe_gain = bf16[1,4096]{1,0:T(2,128)(2,1)} reshape(bf16[4096]{0:T(1024)(128)(2,1)} %param.38) | data formatting | bytes 16384 | tf_op jit(solution)/shard_map/reshape | solution.py:385
  3.2 1.4 %copy.27.routes = s32[64,2]{1,0:T(8,128)} copy(s32[64,2]{0,1:T(2,128)} %param.39) | data formatting | bytes 1024 | tf_op args[17]
  4.6 1.4 %copy.28.route_weight = f32[64,2]{1,0:T(8,128)} copy(f32[64,2]{0,1:T(2,128)} %param.40) | data formatting | bytes 1024 | tf_op args[18]
  6.0 1.9 %copy.25 = f32[16,64,16]{2,1,0:T(8,128)} copy(f32[16,64,16]{1,2,0:T(8,128)} %param.30) | data formatting | bytes 131072 | tf_op args[8]
  7.9 1.9 %copy.26 = f32[16,64,16]{2,1,0:T(8,128)} copy(f32[16,64,16]{1,2,0:T(8,128)} %param.31) | data formatting | bytes 131072 | tf_op args[9]
  9.8 60.9 %shard_map.229 = (bf16[64,512]{1,0:T(8,128)(2,1)}, f32[1024,64]{1,0:T(8,128)}, f32[1024,64]{1,0:T(8,128)}) custom-call(bf16[64,512]{1,0:T(8,128)(2,1)} %tok.1, bf16[1,4096]{1,0:T(2,128)(2,1)} %reshape.45.mix_gain, bf16[1,4096]{1,0:T(2,128)(2,1)} %reshape.46.moe_gain, s32[64,2]{1,0:T(8,128)} %copy.27.routes, f32[64,2]{1,0:T(8,128)} %copy.28.route_weight, ...), custom_call_target="tpu_custom_call" | custom-call | tf_op jit(solution)/shard_map/pallas_call | solution.py:332
  70.7 1.5 %copy.32 = bf16[64,512]{1,0:T(8,128)(2,1)} copy(bf16[64,512]{1,0:T(8,128)(2,1)} %get-tuple-element.12) | data formatting | bytes 131072
  72.2 1.9 %copy.33 = f32[64,16,64]{2,1,0:T(8,128)} copy(f32[64,16,64]{2,1,0:T(8,128)} %bitcast.16) | data formatting | bytes 524288
  74.1 1.9 %copy.34 = f32[64,16,64]{2,1,0:T(8,128)} copy(f32[64,16,64]{2,1,0:T(8,128)} %bitcast.15) | data formatting | bytes 524288

commit v2 on v1

--- a/solution.py
+++ b/solution.py
@@ -29,7 +29,7 @@
     result, new_real, new_imag,
     tok_all, act_all, sib_send_a, sib_recv_a, rem_send_a, rem_recv_a,
     ep_send, frag, acc, sib_send_b, sib_recv_b, rem_send_b, rem_recv_b, ret_send, ret,
-    state_r, state_i, next_r, next_i, pad_r, pad_i, w_in, w_glu, w_out, w_gate, w_up, w_down,
+    state_r, state_i, next_r, next_i, w_in, w_glu, w_out, w_gate, w_up, w_down,
     load_sem, store_sem, s1, r1, s2, r2, s3, r3, s4, r4, s5, r5, s6, r6, s7, r7, s8, r8, s9, r9,
 ):
     e = lax.axis_index("ep")
@@ -41,7 +41,7 @@
     rows, feat = tok.shape
     width = in_weight.shape[0]
     groups, states = eig_real.shape
-    group_width = in_real.shape[1]
+    group_width = width // groups
     exp_dev = gate_weight.shape[0]
     per_ep = exp_dev * capacity
     slots = n_ep * per_ep
@@ -57,7 +57,14 @@
         loads.append(load)
 
     def remote_chip(j):
-        return lax.rem(chip + j, chips)
+        if chips & (chips - 1):
+            return lax.rem(chip + j, chips)
+        other, bit = chip, 1
+        while bit < chips:
+            if j & bit:
+                other = other + bit * (1 - 2 * ((chip // bit) % 2))
+            bit *= 2
+        return other
 
     barrier = pltpu.get_barrier_semaphore()
     greeted = [(e, sib)]
@@ -90,16 +97,6 @@
 
     gather_send(tok, lambda p: tok_all.at[p], lambda i: s1.at[i], lambda p: r1.at[p])
 
-    spread = (
-        lax.broadcasted_iota(jnp.int32, (group_width, width), 1) % group_width
-        == lax.broadcasted_iota(jnp.int32, (group_width, width), 0)
-    ).astype(F32).astype(BF16)
-    own_group = (
-        lax.broadcasted_iota(jnp.int32, (groups * states, width), 1) // group_width
-        == lax.broadcasted_iota(jnp.int32, (groups * states, width), 0) // states
-    )
-    pad_r[...] = jnp.where(own_group, dot_nn(in_real[...].astype(BF16), spread), 0.0).astype(BF16)
-    pad_i[...] = jnp.where(own_group, dot_nn(in_imag[...].astype(BF16), spread), 0.0).astype(BF16)
     square = lax.broadcasted_iota(jnp.int32, (groups, groups), 0) == lax.broadcasted_iota(
         jnp.int32, (groups, groups), 1
     )
@@ -115,9 +112,17 @@
 
     experts = exp_dev * n_ep
     lane_expert = lax.broadcasted_iota(jnp.int32, (rows, experts), 1)
-    route = routes[...]
-    top = route.shape[1]
-    picks = [(route[:, k : k + 1] == lane_expert).astype(F32) for k in range(top)]
+    top = routes.shape[0]
+    token_square = lax.broadcasted_iota(jnp.int32, (rows, rows), 0) == lax.broadcasted_iota(
+        jnp.int32, (rows, rows), 1
+    )
+
+    def column(row):
+        return jnp.sum(jnp.where(token_square, row.astype(F32), 0.0), axis=1, keepdims=True)
+
+    route = [column(routes[k : k + 1, :]).astype(jnp.int32) for k in range(top)]
+    weights = [column(route_weight[k : k + 1, :]) for k in range(top)]
+    picks = [(route[k] == lane_expert).astype(F32) for k in range(top)]
     earlier = (
         lax.broadcasted_iota(jnp.int32, (rows, rows), 0) > lax.broadcasted_iota(jnp.int32, (rows, rows), 1)
     ).astype(F32).astype(BF16)
@@ -126,7 +131,7 @@
     choose = []
     for k in range(top):
         rank = jnp.sum(prefix * picks[k], axis=1, keepdims=True).astype(jnp.int32)
-        slot = route[:, k : k + 1] * capacity + rank
+        slot = route[k] * capacity + rank
         choose.append((slot == lane_slot).astype(F32))
     dispatch = jnp.transpose(sum(choose[1:], choose[0])).astype(BF16)
     choose = [one.astype(BF16) for one in choose]
@@ -134,10 +139,15 @@
     def columns(p):
         return pl.ds(pl.multiple_of(p * feat, feat), feat)
 
+    def gain_row(gain, p):
+        if gain.ndim == 2:
+            return gain[:, columns(p)].astype(F32)
+        return gain[columns(p)].astype(F32).reshape(1, feat)
+
     def in_piece(p, x, total, sq):
         xf = x.astype(F32)
         sq = sq + jnp.sum(xf * xf, axis=1, keepdims=True)
-        y = (xf * mix_gain[:, columns(p)].astype(F32)).astype(BF16)
+        y = (xf * gain_row(mix_gain, p)).astype(BF16)
         return total + dot_nt(y, w_in[:, columns(p)]), sq
 
     loads[0].wait()
@@ -160,12 +170,13 @@
     loads[2].wait()
     readout = skip_weight[...] * driven_f
     c_r, c_i = out_real[...], out_imag[...]
+    b_r, b_i = in_real[...], in_imag[...]
     row_group = lax.broadcasted_iota(jnp.int32, c_r.shape, 0) // group_width
     for g in range(groups):
         at = pl.ds(g, rows, stride=groups)
-        part = slice(g * states, (g + 1) * states)
-        push_r = dot_nt(driven, pad_r[part, :])
-        push_i = dot_nt(driven, pad_i[part, :])
+        mine = row_group == g
+        push_r = dot_nn(driven, jnp.where(mine, b_r, 0.0).astype(BF16))
+        push_i = dot_nn(driven, jnp.where(mine, b_i, 0.0).astype(BF16))
         old_r, old_i = state_r[at, :], state_i[at, :]
         br, bi = bar_r[g : g + 1, :], bar_i[g : g + 1, :]
         fr, fi = fac_r[g : g + 1, :], fac_i[g : g + 1, :]
@@ -173,7 +184,6 @@
         now_i = br * old_i + bi * old_r + (fr * push_i + fi * push_r)
         next_r[at, :] = now_r
         next_i[at, :] = now_i
-        mine = row_group == g
         readout = readout + dot_nt(now_r.astype(BF16), jnp.where(mine, c_r, 0.0).astype(BF16))
         readout = readout - dot_nt(now_i.astype(BF16), jnp.where(mine, c_i, 0.0).astype(BF16))
     activated = jax.nn.gelu(readout).astype(BF16)
@@ -245,7 +255,7 @@
 
     def expert_piece(p, sq, first):
         xf = frag[p].reshape(slots, feat).astype(F32)
-        y = (xf * moe_gain[:, columns(p)].astype(F32)).astype(BF16)
+        y = (xf * gain_row(moe_gain, p)).astype(BF16)
         for x in range(exp_dev):
             gate = dot_nt(y, w_gate[x, :, columns(p)])
             up = dot_nt(y, w_up[x, :, columns(p)])
@@ -296,15 +306,27 @@
         arrive(ret.at[source], s9.at[0], r9.at[source])
     returned = ret[...].reshape(slots, feat)
     total = residual.astype(F32)
-    weights = route_weight[...]
     for k in range(top):
-        total = total + weights[:, k : k + 1] * dot_nn(choose[k], returned)
+        total = total + weights[k] * dot_nn(choose[k], returned)
     result[...] = total.astype(BF16)
 
     for store in stores:
         store.wait()
     for copy in sends:
         copy.wait_send()
+
+
+def hand_over(a, b, c, a_out, b_out, c_out, a_held, b_held, c_held, sem_in, sem_out):
+    triples = ((a, a_held, a_out), (b, b_held, b_out), (c, c_held, c_out))
+    ins = [pltpu.make_async_copy(src, held, sem_in.at[i]) for i, (src, held, _) in enumerate(triples)]
+    outs = [pltpu.make_async_copy(held, dst, sem_out.at[i]) for i, (_, held, dst) in enumerate(triples)]
+    for copy in ins:
+        copy.start()
+    for copy, back in zip(ins, outs):
+        copy.wait()
+        back.start()
+    for back in outs:
+        back.wait()
 
 
 def local(
@@ -329,6 +351,8 @@
     hbm = pl.BlockSpec(memory_space=pl.ANY)
     dma = pltpu.SemaphoreType.DMA
     state_shape = (rows * groups, states)
+    if feat % 256:
+        mix_gain, moe_gain = mix_gain.reshape(1, dim), moe_gain.reshape(1, dim)
     outs = pl.pallas_call(
         functools.partial(layer_kernel, n_ep, n_tp, capacity),
         out_shape=(
@@ -358,8 +382,6 @@
             pltpu.VMEM(state_shape, F32),
             pltpu.VMEM(state_shape, F32),
             pltpu.VMEM(state_shape, F32),
-            pltpu.VMEM((groups * states, width), BF16),
-            pltpu.VMEM((groups * states, width), BF16),
             pltpu.VMEM(in_weight.shape, BF16),
             pltpu.VMEM(glu_weight.shape, BF16),
             pltpu.VMEM(out_weight.shape, BF16),
@@ -382,16 +404,23 @@
             collective_id=0, has_side_effects=True, vmem_limit_bytes=60 * 1024 * 1024
         ),
     )(
-        tokens, mix_gain.reshape(1, dim), moe_gain.reshape(1, dim), routes, route_weight,
+        tokens, mix_gain, moe_gain, routes.T, route_weight.T,
         eig_real, eig_imag, log_step.reshape(1, groups),
-        input_real.reshape(groups * states, group_width),
-        input_imag.reshape(groups * states, group_width),
+        jnp.swapaxes(input_real, 1, 2).reshape(width, states),
+        jnp.swapaxes(input_imag, 1, 2).reshape(width, states),
         output_matrix_real.reshape(width, states), output_matrix_imag.reshape(width, states),
         skip_weight.reshape(1, width), glu_bias.reshape(1, width),
         state_real.reshape(state_shape), state_imag.reshape(state_shape),
         in_weight, glu_weight, out_weight, gate_weight, up_weight, down_weight,
     )
-    result, new_real, new_imag = outs
+    result, new_real, new_imag = pl.pallas_call(
+        hand_over,
+        out_shape=tuple(jax.ShapeDtypeStruct(one.shape, one.dtype) for one in outs),
+        in_specs=[hbm] * 3,
+        out_specs=(hbm,) * 3,
+        scratch_shapes=[pltpu.VMEM(one.shape, one.dtype) for one in outs] + [dma((3,)), dma((3,))],
+        compiler_params=pltpu.CompilerParams(vmem_limit_bytes=60 * 1024 * 1024),
+    )(*outs)
     return result, new_real.reshape(state_real.shape), new_imag.reshape(state_imag.shape)
 
 

time: 76.4 us -> 64.6 us (0.85)
  local copies, waits for them, and re-layouts: 14.4 us -> 0 us
  Pallas kernels: 60.9 us -> 63.8 us
    unnamed x7 -> x0, local copies, waits for them, and re-layouts: 11.8 us -> none
    reshape x2 -> x0, local copies, waits for them, and re-layouts: 2.61 us -> none  [the longest x1 1.31 us: local(): mix_gain.reshape(1, dim)]
    pallas_call x0 -> x1, Pallas kernels: none -> 2.1 us  [local(): pl.pallas_call(hand_over, out_shape=tuple((jax.ShapeDtypeStruct(one.shape...]
    pallas_call x1, Pallas kernels: 60.9 us -> 61.7 us  [local(): pl.pallas_call(functools.partial(layer_kernel, n_ep, n_tp, capacity), out...]
where the time goes in v2:
time: 64.6 us; the launch traced here: 64.4 us
  Pallas kernels  63.8 us (99%)
  between operations  0.65 us (1%)
    pallas_call x1, Pallas kernels, local(): pl.pallas_call(functools.partial(layer_kernel, n_ep, n_tp, capacity), out...  61.7 us
    pallas_call x1, Pallas kernels, local(): pl.pallas_call(hand_over, out_shape=tuple((jax.ShapeDtypeStruct(one.shape...  2.1 us

profile of v2, /device:TPU:0, one launch (start us, length us, event | category | flops | bytes accessed | tf_op | source)
XLA Modules:
  0.0 64.4 jit_solution(6331182263112656991)
XLA Ops:
  0.6 61.7 %shard_map.229 = (bf16[64,512]{1,0:T(8,128)(2,1)}, f32[1024,64]{1,0:T(8,128)}, f32[1024,64]{1,0:T(8,128)}) custom-call(bf16[64,512]{1,0:T(8,128)(2,1)} %tok.1, bf16[4096]{0:T(1024)(128)(2,1)} %mix_gain.1, bf16[4096]{0:T(1024)(128)(2,1)} %moe_gain.1, s32[2,64]{1,0:T(2,128)} %bitcast.23, f32[2,64]{1,0:T(2,128)} %bitcast.24, f32[16,64]{1,0:T(8,128)} %eig_real.1, ...), custom_call_target="tpu_custom_call" | custom-call | tf_op jit(solution)/shard_map/pallas_call | solution.py:356
  62.3 2.1 %shard_map.230 = (bf16[64,512]{1,0:T(8,128)(2,1)}, f32[1024,64]{1,0:T(8,128)}, f32[1024,64]{1,0:T(8,128)}) custom-call(bf16[64,512]{1,0:T(8,128)(2,1)} %get-tuple-element.9.a, f32[1024,64]{1,0:T(8,128)} %get-tuple-element.10.b, f32[1024,64]{1,0:T(8,128)} %get-tuple-element.11.c), custom_call_target="tpu_custom_call" | custom-call | tf_op jit(solution)/shard_map/pallas_call | solution.py:416
